TPU v7x, 32 devices: a whole 2x2x4 slice. The times are simulated.
32 devices in a mesh: grp: 2 (over y), fs: 4 (over z), tp: 4 (over x, core).
Axes of the slice: x: 2, y: 2, z: 4, core: 2. Of those that a mesh axis runs over, the one named last changes fastest.
Arguments:
- tokens: bfloat16 [8192, 2048], P(('grp', 'fs')), parts along dimension 0, may hold values from -6 to 6
- mixer_gain: float32 [2048], replicated, may hold values from 0.1 to 1.9
- outer_weight: float32 [2048, 2048], P('fs', 'tp'), may hold values from -0.125 to 0.125
- inner_weight: float32 [2048, 2048], P('fs', 'tp'), may hold values from -0.125 to 0.125
- value_weight: float32 [2048, 2048], P('fs', 'tp'), may hold values from -0.125 to 0.125
- filter_taps: float32 [3, 2048], P(None, 'tp'), may hold values from -3.5 to 3.5
- mixer_weight: float32 [2048, 2048], P('tp', 'fs'), may hold values from -0.125 to 0.125
- outer_scale: float32 [4, 512], P('tp', 'fs'), may hold values from 0.5 to 2
- inner_scale: float32 [4, 512], P('tp', 'fs'), may hold values from 0.5 to 2
- value_scale: float32 [4, 512], P('tp', 'fs'), may hold values from 0.5 to 2
- mixer_scale: float32 [1, 2048], P(None, 'fs'), may hold values from 0.5 to 2
Outputs:
- layer_out: bfloat16 [8192, 2048], P(('grp', 'fs', 'tp')), parts along dimension 0
There are 2 independent parts, one for each index of `grp`. A program takes and returns all parts, laid end to end along the dimension named above; an argument that names none is the same for every part. Nothing has to cross between parts.
All inputs are finite; a program needn't handle non-finite values.
Results may differ from a plain program's by a relative error of at most 0.014.
Values may be sent and summed in bfloat16 or wider, within the bound.
A program may use at most 64 MiB of HBM per device.

v0:
```python
import functools

import jax
import jax.numpy as jnp
from jax import lax
from jax.experimental import pallas as pl
from jax.experimental.pallas import tpu as pltpu
from jax.sharding import PartitionSpec as P

EPS = 1e-06


def normed(rows, gain):
    values = rows.astype(jnp.float32)
    inverse = lax.rsqrt(jnp.mean(values * values, axis=-1, keepdims=True) + EPS)
    return (values * inverse * gain).astype(jnp.bfloat16)


def rounded(values):
    return lax.optimization_barrier(values.astype(jnp.bfloat16)).astype(jnp.float32)


def add_rows(left, piece):
    return jnp.dot(left, piece, preferred_element_type=jnp.float32)


def per_device(
    tokens,
    mixer_gain,
    outer_weight,
    inner_weight,
    value_weight,
    filter_taps,
    mixer_weight,
    outer_scale,
    inner_scale,
    value_scale,
    mixer_scale,
):
    gathered = (
        lax.all_gather(outer_scale, "fs", axis=1, tiled=True),
        lax.all_gather(inner_scale, "fs", axis=1, tiled=True),
        lax.all_gather(value_scale, "fs", axis=1, tiled=True),
        lax.all_gather(mixer_scale, "fs", axis=1, tiled=True),
    )
    outer_col, inner_col, value_col, mixer_col = [piece.reshape(-1) for piece in gathered]
    seq_rows = tokens.shape[0]
    normal_rows = normed(tokens, mixer_gain)

    def fold_one(piece):
        return add_rows(normal_rows, piece)

    outer_sum = fold_one(
        lax.all_gather(outer_weight.astype(jnp.bfloat16), "fs", axis=0, tiled=True)
    )
    inner_sum = fold_one(
        lax.all_gather(inner_weight.astype(jnp.bfloat16), "fs", axis=0, tiled=True)
    )
    value_sum = fold_one(
        lax.all_gather(value_weight.astype(jnp.bfloat16), "fs", axis=0, tiled=True)
    )
    outer = rounded(outer_sum * outer_col)
    inner = rounded(inner_sum * inner_col)
    value = rounded(value_sum * value_col)
    padded = jnp.pad(inner * value, ((2, 0), (0, 0)))
    filtered = (
        filter_taps[0] * padded[0:seq_rows]
        + filter_taps[1] * padded[1 : seq_rows + 1]
        + filter_taps[2] * padded[2:]
    )
    gated = (outer * filtered).astype(jnp.bfloat16)
    mixer_full = lax.all_gather(mixer_weight.astype(jnp.bfloat16), "fs", axis=1, tiled=True)
    return lax.psum_scatter(
        (jnp.dot(gated, mixer_full, preferred_element_type=jnp.float32) * mixer_col).astype(
            jnp.bfloat16
        ),
        "tp",
        scatter_dimension=0,
        tiled=True,
    )


MESH = pl.DeviceIdType.MESH
MATRICES = 4
SPLIT = 1
PIECES = MATRICES * SPLIT


def mixer_kernel(
    n,
    tokens_hbm,
    gain_ref,
    w0_hbm,
    w1_hbm,
    w2_hbm,
    taps_ref,
    w3_hbm,
    s0_ref,
    s1_ref,
    s2_ref,
    s3_ref,
    out_ref,
    toks,
    rows,
    stage,
    held,
    scales,
    outer_buf,
    inner_buf,
    product,
    gated,
    own_part,
    core_out,
    core_in,
    chip_out,
    chip_in,
    load_sem,
    zl_sem,
    zr_sem,
    zin_sem,
    yout_sem,
    yin_sem,
    sout_sem,
    sin_sem,
    cout_sem,
    cin_sem,
    xout_sem,
    xin_sem,
):
    z = lax.axis_index("fs")
    y = lax.axis_index("grp")
    t = lax.axis_index("tp")
    ntp = 4
    block, width = stage.shape[1], stage.shape[2]
    half = block // 2
    seq = rows.shape[0]
    tile = seq // ntp
    partner = t + 1 - 2 * lax.rem(t, 2)
    across = lax.rem(t + 2, ntp)
    x, core = t // 2, lax.rem(t, 2)
    weights = (w0_hbm, w1_hbm, w2_hbm, w3_hbm)

    loads = [
        pltpu.make_async_copy(weights[m], stage.at[m], load_sem.at[m]) for m in range(MATRICES)
    ]
    token_load = pltpu.make_async_copy(tokens_hbm, toks, load_sem.at[MATRICES])
    for load in loads:
        load.start()
    token_load.start()

    barrier = pltpu.get_barrier_semaphore()
    for d in range(1, n):
        pl.semaphore_signal(
            barrier, inc=1, device_id={"fs": lax.rem(z + d, n)}, device_id_type=MESH
        )
    for d in range(1, ntp):
        pl.semaphore_signal(
            barrier, inc=1, device_id={"tp": lax.rem(t + d, ntp)}, device_id_type=MESH
        )
    pl.semaphore_signal(barrier, inc=1, device_id={"grp": 1 - y}, device_id_type=MESH)

    q = s0_ref.shape[1]
    scales[z, :, 0:q] = s0_ref[...]
    scales[z, :, q : 2 * q] = s1_ref[...]
    scales[z, :, 2 * q : 3 * q] = s2_ref[...]
    scales[z, :, 3 * q :] = s3_ref[...]

    def cast(m):
        loads[m].wait()
        held[m, pl.ds(pl.multiple_of(z * block, block), block), :] = stage[m].astype(jnp.bfloat16)

    chunk = half // SPLIT

    def rows_of(p, b, side):
        first = b * block + side * half + (p % SPLIT) * chunk
        return held.at[p // SPLIT, pl.ds(pl.multiple_of(first, chunk), chunk), :]

    def part_of(p, b):
        return rows_of(p, b, y)

    def other_of(p, b):
        return rows_of(p, b, 1 - y)

    def to_left(m, b):
        return pltpu.make_async_remote_copy(
            src_ref=part_of(m, b),
            dst_ref=part_of(m, b),
            send_sem=zl_sem.at[m, b],
            recv_sem=zin_sem.at[m, b],
            device_id={"fs": z - 1},
            device_id_type=MESH,
        )

    def to_right(m, b):
        return pltpu.make_async_remote_copy(
            src_ref=part_of(m, b),
            dst_ref=part_of(m, b),
            send_sem=zr_sem.at[m, b],
            recv_sem=zin_sem.at[m, b],
            device_id={"fs": z + 1},
            device_id_type=MESH,
        )

    def to_twin(m, b):
        return pltpu.make_async_remote_copy(
            src_ref=part_of(m, b),
            dst_ref=part_of(m, b),
            send_sem=yout_sem.at[m, b],
            recv_sem=yin_sem.at[m, b],
            device_id={"grp": 1 - y},
            device_id_type=MESH,
        )

    def from_twin(m, b):
        return pltpu.make_async_remote_copy(
            src_ref=other_of(m, b),
            dst_ref=other_of(m, b),
            send_sem=yout_sem.at[m, b],
            recv_sem=yin_sem.at[m, b],
            device_id={"grp": 1 - y},
            device_id_type=MESH,
        )

    def scale_copy(d):
        return pltpu.make_async_remote_copy(
            src_ref=scales.at[z],
            dst_ref=scales.at[z],
            send_sem=sout_sem.at[d],
            recv_sem=sin_sem.at[z],
            device_id={"fs": lax.rem(z + d, n)},
            device_id_type=MESH,
        )

    def scale_arrival(d):
        source = lax.rem(z + d, n)
        return pltpu.make_async_remote_copy(
            src_ref=scales.at[source],
            dst_ref=scales.at[source],
            send_sem=sout_sem.at[d],
            recv_sem=sin_sem.at[source],
            device_id={"fs": source},
            device_id_type=MESH,
        )

    def send_own(m):
        @pl.when(z >= 1)
        def _():
            to_left(m, z).start()

        @pl.when(z <= n - 2)
        def _():
            to_right(m, z).start()

    def relay(m, s):
        from_right, from_left = z + 1 + s, z - 1 - s

        @pl.when(from_right <= n - 1)
        def _():
            to_left(m, from_right).wait_recv()

            @pl.when(z >= 1)
            def _():
                to_left(m, from_right).start()

            to_twin(m, from_right).start()

        @pl.when(from_left >= 0)
        def _():
            to_right(m, from_left).wait_recv()

            @pl.when(z <= n - 2)
            def _():
                to_right(m, from_left).start()

            to_twin(m, from_left).start()

    def twin_arrival(m, s):
        @pl.when(z + 1 + s <= n - 1)
        def _():
            from_twin(m, z + 1 + s).wait_recv()

        @pl.when(z - 1 - s >= 0)
        def _():
            from_twin(m, z - 1 - s).wait_recv()

    def column(k):
        return jnp.concatenate([scales[b, :, k * q : (k + 1) * q] for b in range(n)], axis=1)

    def project(m, first, count):
        return jnp.dot(
            rows[first : first + count, :], held[m], preferred_element_type=jnp.float32
        ) * column(m)

    def project_tiles(m, target, start, stop):
        for i in range(start, stop):
            first = i * tile
            target[first : first + tile, :] = project(m, first, tile).astype(jnp.bfloat16)

    cast(0)
    cast(1)
    pl.semaphore_wait(barrier, n - 1 + ntp - 1 + 1)
    for d in range(1, n):
        scale_copy(d).start()
    send_own(0)
    cast(2)
    cast(3)
    at_end = (z == 0) | (z == n - 1)

    @pl.when(at_end)
    def _():
        for p in range(1, PIECES):
            send_own(p)

    def send_own_inside(m):
        @pl.when(jnp.logical_not(at_end))
        def _():
            send_own(m)

    token_load.wait()
    strip = seq // 8

    @pl.loop(0, 8)
    def _(i):
        at = pl.ds(pl.multiple_of(i * strip, strip), strip)
        rows[at, :] = normed(toks[at, :], gain_ref[...])

    product[0:8, :] = jnp.zeros((8, width), jnp.float32)

    def gate_tile(i):
        first = i * tile
        value = project(2, first, tile).astype(jnp.bfloat16).astype(jnp.float32)
        product[8 + first : 8 + first + tile, :] = (
            inner_buf[first : first + tile, :].astype(jnp.float32) * value
        )
        filtered = (
            taps_ref[0:1, :] * product[6 + first : 6 + first + tile, :]
            + taps_ref[1:2, :] * product[7 + first : 7 + first + tile, :]
            + taps_ref[2:3, :] * product[8 + first : 8 + first + tile, :]
        )
        outer = outer_buf[first : first + tile, :].astype(jnp.float32)
        gated[first : first + tile, :] = (outer * filtered).astype(jnp.bfloat16)

    def core_copy(b):
        return pltpu.make_async_remote_copy(
            src_ref=core_out.at[b],
            dst_ref=core_in.at[b],
            send_sem=cout_sem.at[b],
            recv_sem=cin_sem.at[b],
            device_id={"tp": partner},
            device_id_type=MESH,
        )

    def chip_copy(b):
        return pltpu.make_async_remote_copy(
            src_ref=chip_out.at[b],
            dst_ref=chip_in.at[b],
            send_sem=xout_sem.at[b],
            recv_sem=xin_sem.at[b],
            device_id={"tp": across},
            device_id_type=MESH,
        )

    def mix_rows(b, index):
        at = pl.ds(pl.multiple_of(index * tile, tile), tile)
        weight = held[3, pl.ds(pl.multiple_of(b * block, block), block), :]
        return (
            jnp.dot(gated[at, :], weight, preferred_element_type=jnp.float32)
            * scales[b, :, 3 * q :]
        )

    def mix(b):
        for k in range(2):
            core_out[b, k] = mix_rows(b, 2 * k + 1 - core).astype(jnp.bfloat16)
        core_copy(b).start()
        for k in range(2):
            own_part[b, k] = mix_rows(b, 2 * k + core)
        core_copy(b).wait_recv()
        chip_out[b] = (own_part[b, 1 - x] + core_in[b, 1 - x].astype(jnp.float32)).astype(
            jnp.bfloat16
        )
        chip_copy(b).start()

    def mix_arrived(s):
        @pl.loop(0, 2)
        def _(side):
            b = z + (1 + s) * (1 - 2 * side)

            @pl.when((b >= 0) & (b <= n - 1))
            def _():
                for p in range(3 * SPLIT, PIECES):
                    from_twin(p, b).wait_recv()
                mix(b)

    def all_twins(m):
        for p in range(m * SPLIT, (m + 1) * SPLIT):
            for s in range(n - 1):
                twin_arrival(p, s)

    def outer_tiles(start, stop):
        project_tiles(0, outer_buf, start, stop)

    def inner_tiles(start, stop):
        project_tiles(1, inner_buf, start, stop)

    def scales_in():
        for d in range(1, n):
            scale_arrival(d).wait_recv()

    steps = [(p, s) for p in range(PIECES) for s in range(n - 1)]
    per_matrix = SPLIT * (n - 1)
    work = {
        per_matrix + SPLIT: [
            scales_in,
            functools.partial(all_twins, 0),
            functools.partial(outer_tiles, 0, 2),
        ],
        per_matrix + 2 * SPLIT: [functools.partial(outer_tiles, 2, 4)],
        2 * per_matrix + SPLIT: [
            functools.partial(all_twins, 1),
            functools.partial(inner_tiles, 0, 2),
        ],
        2 * per_matrix + 2 * SPLIT: [functools.partial(inner_tiles, 2, 4)],
        3 * per_matrix: [functools.partial(all_twins, 2)]
        + [functools.partial(gate_tile, i) for i in range(4)]
        + [functools.partial(mix, z)],
    }
    for at, (p, s) in enumerate(steps):
        relay(p, s)
        if s == n - 3 and p < PIECES - 1:
            send_own_inside(p + 1)
        for task in work.get(at, ()):
            task()
        if p == PIECES - 1 and s >= 1:
            mix_arrived(s - 1)
    mix_arrived(n - 2)

    @pl.loop(0, n)
    def _(b):
        chip_copy(b).wait_recv()
        out_ref[:, pl.ds(pl.multiple_of(b * width, width), width)] = (
            own_part[b, x]
            + core_in[b, x].astype(jnp.float32)
            + chip_in[b].astype(jnp.float32)
        ).astype(jnp.bfloat16)
        core_copy(b).wait_send()
        chip_copy(b).wait_send()

    for d in range(1, n):
        scale_copy(d).wait_send()
    for p in range(PIECES):

        @pl.loop(0, n)
        def _(b):
            @pl.when((b >= z) & (z >= 1))
            def _():
                to_left(p, b).wait_send()

            @pl.when((b <= z) & (z <= n - 2))
            def _():
                to_right(p, b).wait_send()

            @pl.when(b != z)
            def _():
                to_twin(p, b).wait_send()


def fused_device(
    n,
    tokens,
    mixer_gain,
    outer_weight,
    inner_weight,
    value_weight,
    filter_taps,
    mixer_weight,
    outer_scale,
    inner_scale,
    value_scale,
    mixer_scale,
):
    seq, depth = tokens.shape
    block, width = outer_weight.shape
    tile = seq // 4
    whole = pl.BlockSpec(memory_space=pltpu.VMEM)
    anywhere = pl.BlockSpec(memory_space=pl.ANY)
    bf16, f32 = jnp.bfloat16, jnp.float32
    dma = pltpu.SemaphoreType.DMA
    scale_width = 3 * outer_scale.shape[1] + mixer_scale.shape[1]
    return pl.pallas_call(
        functools.partial(mixer_kernel, n),
        out_shape=jax.ShapeDtypeStruct((tile, n * width), bf16),
        in_specs=[
            anywhere,
            whole,
            anywhere,
            anywhere,
            anywhere,
            whole,
            anywhere,
            whole,
            whole,
            whole,
            whole,
        ],
        out_specs=whole,
        scratch_shapes=[
            pltpu.VMEM((seq, depth), bf16),
            pltpu.VMEM((seq, depth), bf16),
            pltpu.VMEM((MATRICES, block, width), f32),
            pltpu.VMEM((MATRICES, n * block, width), bf16),
            pltpu.VMEM((n, 1, scale_width), f32),
            pltpu.VMEM((seq, width), bf16),
            pltpu.VMEM((seq, width), bf16),
            pltpu.VMEM((seq + 8, width), f32),
            pltpu.VMEM((seq, width), bf16),
            pltpu.VMEM((n, 2, tile, width), f32),
            pltpu.VMEM((n, 2, tile, width), bf16),
            pltpu.VMEM((n, 2, tile, width), bf16),
            pltpu.VMEM((n, tile, width), bf16),
            pltpu.VMEM((n, tile, width), bf16),
            dma((MATRICES + 1,)),
            dma((PIECES, n)),
            dma((PIECES, n)),
            dma((PIECES, n)),
            dma((PIECES, n)),
            dma((PIECES, n)),
            dma((n,)),
            dma((n,)),
            dma((n,)),
            dma((n,)),
            dma((n,)),
            dma((n,)),
        ],
        compiler_params=pltpu.CompilerParams(
            collective_id=0, has_side_effects=True, vmem_limit_bytes=56 * 2**20
        ),
    )(
        tokens,
        mixer_gain.reshape(1, -1),
        outer_weight,
        inner_weight,
        value_weight,
        filter_taps,
        mixer_weight,
        outer_scale,
        inner_scale,
        value_scale,
        mixer_scale,
    )


def choose(mesh):
    n, ntp, groups = mesh.shape["fs"], mesh.shape["tp"], mesh.shape["grp"]

    def run(*args):
        tokens, weight, mixer, scale = args[0], args[2], args[6], args[7]
        fits = (
            groups == 2
            and ntp == 4
            and n == 4
            and weight.shape == mixer.shape
            and weight.shape[0] % (32 * SPLIT) == 0
            and weight.shape[1] % 128 == 0
            and scale.shape[1] % 128 == 0
            and tokens.shape[0] % 256 == 0
        )
        return fused_device(n, *args) if fits else per_device(*args)

    return run


def solution(mesh):
    in_specs = (
        P(("grp", "fs"), None),
        P(),
        P("fs", "tp"),
        P("fs", "tp"),
        P("fs", "tp"),
        P(None, "tp"),
        P("tp", "fs"),
        P("tp", "fs"),
        P("tp", "fs"),
        P("tp", "fs"),
        P(None, "fs"),
    )
    out_specs = P(("grp", "fs", "tp"), None)
    return jax.shard_map(
        choose(mesh), mesh=mesh, in_specs=in_specs, out_specs=out_specs, check_vma=False
    )
```

profile of v0, /device:TPU:0, one launch (start us, length us, event | category | flops | bytes accessed | tf_op | source)
XLA Modules:
  0.0 101.9 jit_solution(6048983563544582661)
XLA Ops:
  0.0 99.6 %shard_map.109 = bf16[256,2048]{1,0:T(8,128)(2,1)} custom-call(bf16[1024,2048]{1,0:T(8,128)(2,1)} %tokens_hbm.1, f32[1,2048]{1,0:T(1,128)} %bitcast.1, f32[512,512]{1,0:T(8,128)} %w0_hbm.1, f32[512,512]{1,0:T(8,128)} %w1_hbm.1, f32[512,512]{1,0:T(8,128)} %w2_hbm.1, f32[3,512]{1,0:T(4,128)} %taps_ref.1, f32[512,512]{1,0:T(8,128)} %w3_hbm.1, f32[1,128]{1,0:T(1,128)} %s0_ref.1, ...), custom_call_target="tpu_custom_call" | custom-call | tf_op jit(solution)/shard_map/pallas_call | solution.py:489
  99.6 2.3 %copy.13 = bf16[256,2048]{1,0:T(8,128)(2,1)} copy(bf16[256,2048]{1,0:T(8,128)(2,1)} %shard_map.109) | data formatting | bytes 2097152
where the time goes:
time: 102 us
  Pallas kernels  99.6 us (98%)
  local copies, waits for them, and re-layouts  2.3 us (2%)
    pallas_call x1, Pallas kernels, fused_device(): pl.pallas_call(functools.partial(mixer_kernel, n), out_shape=jax.ShapeDty...  99.6 us
    unnamed x1, local copies, waits for them, and re-layouts  2.3 us

commit v1 on v0

v1 whole, which is shorter than its diff:
```python
import functools

import jax
import jax.numpy as jnp
from jax import lax
from jax.experimental import pallas as pl
from jax.experimental.pallas import tpu as pltpu
from jax.sharding import PartitionSpec as P

EPS = 1e-06


def normed(rows, gain):
    values = rows.astype(jnp.float32)
    inverse = lax.rsqrt(jnp.mean(values * values, axis=-1, keepdims=True) + EPS)
    return (values * inverse * gain).astype(jnp.bfloat16)


def rounded(values):
    return lax.optimization_barrier(values.astype(jnp.bfloat16)).astype(jnp.float32)


def add_rows(left, piece):
    return jnp.dot(left, piece, preferred_element_type=jnp.float32)


def per_device(
    tokens,
    mixer_gain,
    outer_weight,
    inner_weight,
    value_weight,
    filter_taps,
    mixer_weight,
    outer_scale,
    inner_scale,
    value_scale,
    mixer_scale,
):
    gathered = (
        lax.all_gather(outer_scale, "fs", axis=1, tiled=True),
        lax.all_gather(inner_scale, "fs", axis=1, tiled=True),
        lax.all_gather(value_scale, "fs", axis=1, tiled=True),
        lax.all_gather(mixer_scale, "fs", axis=1, tiled=True),
    )
    outer_col, inner_col, value_col, mixer_col = [piece.reshape(-1) for piece in gathered]
    seq_rows = tokens.shape[0]
    normal_rows = normed(tokens, mixer_gain)

    def fold_one(piece):
        return add_rows(normal_rows, piece)

    outer_sum = fold_one(
        lax.all_gather(outer_weight.astype(jnp.bfloat16), "fs", axis=0, tiled=True)
    )
    inner_sum = fold_one(
        lax.all_gather(inner_weight.astype(jnp.bfloat16), "fs", axis=0, tiled=True)
    )
    value_sum = fold_one(
        lax.all_gather(value_weight.astype(jnp.bfloat16), "fs", axis=0, tiled=True)
    )
    outer = rounded(outer_sum * outer_col)
    inner = rounded(inner_sum * inner_col)
    value = rounded(value_sum * value_col)
    padded = jnp.pad(inner * value, ((2, 0), (0, 0)))
    filtered = (
        filter_taps[0] * padded[0:seq_rows]
        + filter_taps[1] * padded[1 : seq_rows + 1]
        + filter_taps[2] * padded[2:]
    )
    gated = (outer * filtered).astype(jnp.bfloat16)
    mixer_full = lax.all_gather(mixer_weight.astype(jnp.bfloat16), "fs", axis=1, tiled=True)
    return lax.psum_scatter(
        (jnp.dot(gated, mixer_full, preferred_element_type=jnp.float32) * mixer_col).astype(
            jnp.bfloat16
        ),
        "tp",
        scatter_dimension=0,
        tiled=True,
    )


MESH = pl.DeviceIdType.MESH
MATRICES = 3
EARLY = 2


def mixer_kernel(
    n,
    tokens_hbm,
    gain_ref,
    w0_hbm,
    w1_hbm,
    w2_hbm,
    taps_ref,
    w3_hbm,
    s0_ref,
    s1_ref,
    s2_ref,
    s3_ref,
    out_ref,
    toks,
    rows,
    stage,
    held,
    mix,
    scales,
    acc,
    product,
    gated,
    gates_in,
    mixed,
    load_sem,
    zl_sem,
    zr_sem,
    zin_sem,
    yout_sem,
    yin_sem,
    dout_sem,
    din_sem,
    sout_sem,
    sin_sem,
    xout_sem,
    xin_sem,
    cout_sem,
    cin_sem,
    rout_sem,
    rin_sem,
    gout_sem,
    gin_sem,
):
    z = lax.axis_index("fs")
    y = lax.axis_index("grp")
    t = lax.axis_index("tp")
    ntp = 4
    block = stage.shape[1]
    half = block // 2
    seq = rows.shape[0]
    tile = seq // ntp
    q = s0_ref.shape[1]
    pieces = EARLY + n
    partner = t + 1 - 2 * lax.rem(t, 2)
    across = lax.rem(t + 2, ntp)
    corner = lax.rem(partner + 2, ntp)
    peers = (partner, across, corner)
    weights = (w0_hbm, w1_hbm, w2_hbm, w3_hbm)

    loads = [
        pltpu.make_async_copy(weights[m], stage.at[m], load_sem.at[m]) for m in range(MATRICES + 1)
    ]
    token_load = pltpu.make_async_copy(tokens_hbm, toks, load_sem.at[MATRICES + 1])
    loads[MATRICES].start()
    for m in range(MATRICES):
        loads[m].start()
    token_load.start()

    barrier = pltpu.get_barrier_semaphore()
    for d in range(1, n):
        pl.semaphore_signal(
            barrier, inc=1, device_id={"fs": lax.rem(z + d, n)}, device_id_type=MESH
        )
    for d in range(1, ntp):
        pl.semaphore_signal(
            barrier, inc=1, device_id={"tp": lax.rem(t + d, ntp)}, device_id_type=MESH
        )
    pl.semaphore_signal(barrier, inc=1, device_id={"grp": 1 - y}, device_id_type=MESH)

    scales[z, :, 0:q] = s0_ref[...]
    scales[z, :, q : 2 * q] = s1_ref[...]
    scales[z, :, 2 * q : 3 * q] = s2_ref[...]
    scales[z, :, 3 * q :] = s3_ref[...]

    def piece(p, b, side):
        if p < EARLY:
            return mix.at[b, EARLY * side + p, t]
        first = pl.multiple_of(b * block + side * half, half)
        return held.at[p - EARLY, pl.ds(first, half), :]

    def remote(ref, send, recv, target):
        return pltpu.make_async_remote_copy(
            src_ref=ref,
            dst_ref=ref,
            send_sem=send,
            recv_sem=recv,
            device_id=target,
            device_id_type=MESH,
        )

    def to_left(p, b):
        return remote(piece(p, b, y), zl_sem.at[p, b], zin_sem.at[p, b], {"fs": z - 1})

    def to_right(p, b):
        return remote(piece(p, b, y), zr_sem.at[p, b], zin_sem.at[p, b], {"fs": z + 1})

    def to_twin(p, b):
        return remote(piece(p, b, y), yout_sem.at[p, b], yin_sem.at[p, b], {"grp": 1 - y})

    def from_twin(p, b):
        return remote(piece(p, b, 1 - y), yout_sem.at[p, b], yin_sem.at[p, b], {"grp": 1 - y})

    inward = jnp.where(z == 0, 1, n - 2)

    def second_half(p, b):
        return remote(piece(p, b, 1 - y), dout_sem.at[p], din_sem.at[p], {"fs": inward})

    def direct(b):
        return ((z == 1) & (b == 0)) | ((z == n - 2) & (b == n - 1))

    at_end = (z == 0) | (z == n - 1)

    def scale_copy(d):
        return remote(scales.at[z], sout_sem.at[d], sin_sem.at[z], {"fs": lax.rem(z + d, n)})

    def scale_arrival(d):
        source = lax.rem(z + d, n)
        return remote(scales.at[source], sout_sem.at[d], sin_sem.at[source], {"fs": source})

    def send_own(p):
        @pl.when(z >= 1)
        def _():
            to_left(p, z).start()

        @pl.when(z <= n - 2)
        def _():
            to_right(p, z).start()

        @pl.when(at_end)
        def _():
            second_half(p, z).start()

    def relay(p, s):
        from_right, from_left = z + 1 + s, z - 1 - s

        @pl.when(from_right <= n - 1)
        def _():
            to_left(p, from_right).wait_recv()

            @pl.when(z >= 1)
            def _():
                to_left(p, from_right).start()

            @pl.when(jnp.logical_not(direct(from_right)))
            def _():
                to_twin(p, from_right).start()

        @pl.when(from_left >= 0)
        def _():
            to_right(p, from_left).wait_recv()

            @pl.when(z <= n - 2)
            def _():
                to_right(p, from_left).start()

            @pl.when(jnp.logical_not(direct(from_left)))
            def _():
                to_twin(p, from_left).start()

    def second_arrived(p, b):
        @pl.when(direct(b))
        def _():
            second_half(p, b).wait_recv()

        @pl.when(jnp.logical_not(direct(b)))
        def _():
            from_twin(p, b).wait_recv()

    def each_block(s, act):
        @pl.loop(0, 2)
        def _(side):
            b = z + (1 + s) * (1 - 2 * side)

            @pl.when((b >= 0) & (b <= n - 1))
            def _():
                act(b)

    def across_copy(b):
        return remote(mix.at[b, :, t], xout_sem.at[b], xin_sem.at[b], {"tp": across})

    def across_arrival(b):
        return remote(mix.at[b, :, across], xout_sem.at[b], xin_sem.at[b], {"tp": across})

    def core_copy(b):
        return remote(mix.at[b, :, t], cout_sem.at[b], cin_sem.at[b], {"tp": partner})

    def core_arrival(b):
        return remote(mix.at[b, :, partner], cout_sem.at[b], cin_sem.at[b], {"tp": partner})

    def core_relay(b):
        return remote(mix.at[b, :, across], rout_sem.at[b], rin_sem.at[b], {"tp": partner})

    def core_relay_arrival(b):
        return remote(mix.at[b, :, corner], rout_sem.at[b], rin_sem.at[b], {"tp": partner})

    def spread(b):
        across_copy(b).start()
        core_copy(b).start()

    def spread_arrived(s):
        def act(b):
            for p in range(EARLY):
                second_arrived(p, b)
            spread(b)

        each_block(s, act)

    def pass_on(b):
        across_arrival(b).wait_recv()
        core_relay(b).start()

    def multiply(c, b, first_time=False):
        at = pl.ds(pl.multiple_of(b * block, block), block)
        for i in range(2):
            r = slice(i * seq // 2, (i + 1) * seq // 2)
            part = jnp.dot(rows[r, at], held[c, at, :], preferred_element_type=jnp.float32)
            acc[c, r, :] = part if first_time else acc[c, r, :] + part

    def multiply_arrived(c, s):
        def act(b):
            second_arrived(EARLY + c, b)
            multiply(c, b)

        each_block(s, act)

    def gate_copy(c, k):
        return pltpu.make_async_remote_copy(
            src_ref=gated.at[c, pl.ds(pl.multiple_of(peers[k] * tile, tile), tile), :],
            dst_ref=gates_in.at[c, t],
            send_sem=gout_sem.at[c, k],
            recv_sem=gin_sem.at[c, k],
            device_id={"tp": peers[k]},
            device_id_type=MESH,
        )

    def gate_arrival(c, k):
        return remote(gates_in.at[c, peers[k]], gout_sem.at[c, k], gin_sem.at[c, k], {"tp": peers[k]})

    def gate(c):
        col = scales[c, :, 0 : 3 * q]
        lanes = slice(c * q, (c + 1) * q)

        def scaled(m):
            part = acc[c, :, m * q : (m + 1) * q] * col[:, m * q : (m + 1) * q]
            return part.astype(jnp.bfloat16).astype(jnp.float32)

        product[8:, :] = scaled(1) * scaled(2)
        filtered = (
            taps_ref[0:1, lanes] * product[6 : 6 + seq, :]
            + taps_ref[1:2, lanes] * product[7 : 7 + seq, :]
            + taps_ref[2:3, lanes] * product[8 : 8 + seq, :]
        )
        gated[c] = (scaled(0) * filtered).astype(jnp.bfloat16)
        for k in (2, 1, 0):
            gate_copy(c, k).start()
        gates_in[c, t] = gated[c, pl.ds(pl.multiple_of(t * tile, tile), tile), :]

    def gates_arrived(c):
        for k in range(ntp - 1):
            gate_arrival(c, k).wait_recv()

    def mix_chunks(first, last, final):
        count = last - first
        left = jnp.concatenate(
            [gates_in[c, k] for c in range(first, last) for k in range(ntp)], axis=1
        )
        for b in range(n):
            cols = slice(b * block, (b + 1) * block)
            right = mix[b, first:last].reshape(count * ntp * q, block)
            part = jnp.dot(left, right, preferred_element_type=jnp.float32)
            if final:
                out_ref[:, cols] = ((mixed[:, cols] + part) * scales[b, :, 3 * q :]).astype(
                    jnp.bfloat16
                )
            else:
                mixed[:, cols] = part

    def mix_in():
        @pl.loop(0, n)
        def _(b):
            core_arrival(b).wait_recv()
            core_relay_arrival(b).wait_recv()

    strip = seq // 8

    def normalise(i):
        at = slice(i * strip, (i + 1) * strip)
        rows[at, :] = normed(toks[at, :], gain_ref[...])

    loads[MATRICES].wait()
    for c in range(n):
        mix[z, c, t] = stage[MATRICES, c * q : (c + 1) * q, :].astype(jnp.bfloat16)
    pl.semaphore_wait(barrier, n - 1 + ntp - 1 + 1)
    for p in range(EARLY):
        send_own(p)
    for d in range(1, n):
        scale_copy(d).start()
    spread(z)
    for m in range(MATRICES):
        loads[m].wait()
        for c in range(n):
            held[c, pl.ds(pl.multiple_of(z * block, block), block), m * q : (m + 1) * q] = stage[
                m, :, c * q : (c + 1) * q
            ].astype(jnp.bfloat16)
    product[0:8, :] = jnp.zeros((8, q), jnp.float32)

    @pl.when(at_end)
    def _():
        for p in range(EARLY, pieces):
            send_own(p)

    def send_own_inside(p):
        @pl.when(jnp.logical_not(at_end))
        def _():
            send_own(p)

    token_load.wait()

    def own_part(c):
        multiply(c, z, True)

    def scales_in():
        for d in range(1, n):
            scale_arrival(d).wait_recv()

    part = functools.partial
    hops = n - 1
    work = {k: [] for k in range(pieces * hops)}
    for i in range(8):
        work[i // 2].append(part(normalise, i))
    for c in range(n):
        work[4 + c // 2].append(part(own_part, c))
    for s in range(hops):
        work[hops * EARLY - 1 + s].append(part(spread_arrived, s))
    work[7].append(scales_in)
    for c in range(n):
        for s in range(hops):
            at = (EARLY + c) * hops + s + 1
            if at in work:
                work[at].append(part(multiply_arrived, c, s))
                if s == hops - 1:
                    work[at].append(part(gate, c))
    work[9].append(lambda: pass_on(z))
    work[12].append(lambda: each_block(0, pass_on))
    work[14].append(lambda: each_block(1, pass_on))
    work[15].append(lambda: each_block(2, pass_on))
    work[16] += [mix_in, part(gates_arrived, 0), part(gates_arrived, 1), part(mix_chunks, 0, 2, False)]

    for k in range(pieces * hops):
        p, s = divmod(k, hops)
        relay(p, s)
        if s == n - 3 and p + 1 < pieces and p + 1 >= EARLY:
            send_own_inside(p + 1)
        for task in work[k]:
            task()
    multiply_arrived(n - 1, hops - 1)
    gate(n - 1)
    gates_arrived(n - 2)
    gates_arrived(n - 1)
    mix_chunks(n - 2, n, True)

    for d in range(1, n):
        scale_copy(d).wait_send()
    for c in range(n):
        for k in range(ntp - 1):
            gate_copy(c, k).wait_send()

    @pl.loop(0, n)
    def _(b):
        across_copy(b).wait_send()
        core_copy(b).wait_send()
        core_relay(b).wait_send()

    for p in range(pieces):

        @pl.when(at_end)
        def _():
            second_half(p, z).wait_send()

        @pl.loop(0, n)
        def _(b):
            @pl.when((b >= z) & (z >= 1))
            def _():
                to_left(p, b).wait_send()

            @pl.when((b <= z) & (z <= n - 2))
            def _():
                to_right(p, b).wait_send()

            @pl.when((b != z) & jnp.logical_not(direct(b)))
            def _():
                to_twin(p, b).wait_send()


def fused_device(
    n,
    tokens,
    mixer_gain,
    outer_weight,
    inner_weight,
    value_weight,
    filter_taps,
    mixer_weight,
    outer_scale,
    inner_scale,
    value_scale,
    mixer_scale,
):
    ntp = 4
    seq, depth = tokens.shape
    block, width = outer_weight.shape
    tile = seq // ntp
    q = outer_scale.shape[1]
    pieces = EARLY + n
    whole = pl.BlockSpec(memory_space=pltpu.VMEM)
    anywhere = pl.BlockSpec(memory_space=pl.ANY)
    bf16, f32 = jnp.bfloat16, jnp.float32
    dma = pltpu.SemaphoreType.DMA
    scale_width = 3 * q + mixer_scale.shape[1]
    return pl.pallas_call(
        functools.partial(mixer_kernel, n),
        out_shape=jax.ShapeDtypeStruct((tile, n * block), bf16),
        in_specs=[
            anywhere,
            whole,
            anywhere,
            anywhere,
            anywhere,
            whole,
            anywhere,
            whole,
            whole,
            whole,
            whole,
        ],
        out_specs=whole,
        scratch_shapes=[
            pltpu.VMEM((seq, depth), bf16),
            pltpu.VMEM((seq, depth), bf16),
            pltpu.VMEM((MATRICES + 1, block, width), f32),
            pltpu.VMEM((n, depth, MATRICES * q), bf16),
            pltpu.VMEM((n, n, ntp, q, block), bf16),
            pltpu.VMEM((n, 1, scale_width), f32),
            pltpu.VMEM((n, seq, MATRICES * q), f32),
            pltpu.VMEM((seq + 8, q), f32),
            pltpu.VMEM((n, seq, q), bf16),
            pltpu.VMEM((n, ntp, tile, q), bf16),
            pltpu.VMEM((tile, n * block), f32),
            dma((MATRICES + 2,)),
            dma((pieces, n)),
            dma((pieces, n)),
            dma((pieces, n)),
            dma((pieces, n)),
            dma((pieces, n)),
            dma((pieces,)),
            dma((pieces,)),
            dma((n,)),
            dma((n,)),
            dma((n,)),
            dma((n,)),
            dma((n,)),
            dma((n,)),
            dma((n,)),
            dma((n,)),
            dma((n, ntp - 1)),
            dma((n, ntp - 1)),
        ],
        compiler_params=pltpu.CompilerParams(
            collective_id=0, has_side_effects=True, vmem_limit_bytes=60 * 2**20
        ),
    )(
        tokens,
        mixer_gain.reshape(1, -1),
        outer_weight,
        inner_weight,
        value_weight,
        filter_taps,
        mixer_weight,
        outer_scale,
        inner_scale,
        value_scale,
        mixer_scale,
    )


def choose(mesh):
    n, ntp, groups = mesh.shape["fs"], mesh.shape["tp"], mesh.shape["grp"]

    def run(*args):
        tokens, weight, mixer, scale = args[0], args[2], args[6], args[7]
        fits = (
            groups == 2
            and ntp == 4
            and n == 4
            and weight.shape == mixer.shape
            and weight.shape[0] == n * scale.shape[1]
            and scale.shape[1] % 128 == 0
            and tokens.shape[0] % 256 == 0
        )
        return fused_device(n, *args) if fits else per_device(*args)

    return run


def solution(mesh):
    in_specs = (
        P(("grp", "fs"), None),
        P(),
        P("fs", "tp"),
        P("fs", "tp"),
        P("fs", "tp"),
        P(None, "tp"),
        P("tp", "fs"),
        P("tp", "fs"),
        P("tp", "fs"),
        P("tp", "fs"),
        P(None, "fs"),
    )
    out_specs = P(("grp", "fs", "tp"), None)
    return jax.shard_map(
        choose(mesh), mesh=mesh, in_specs=in_specs, out_specs=out_specs, check_vma=False
    )
```

time: 102 us -> 94.7 us (0.928)
  Pallas kernels: 99.6 us -> 92.1 us
    pallas_call x1, Pallas kernels: 99.6 us -> 92.1 us  [fused_device(): pl.pallas_call(functools.partial(mixer_kernel, n), out_shape=jax.ShapeDty...]
where the time goes in v1:
time: 94.7 us; the launch traced here: 94.4 us
  Pallas kernels  92.1 us (97%)
  local copies, waits for them, and re-layouts  2.3 us (2%)
    pallas_call x1, Pallas kernels, fused_device(): pl.pallas_call(functools.partial(mixer_kernel, n), out_shape=jax.ShapeDty...  92.1 us
    unnamed x1, local copies, waits for them, and re-layouts  2.3 us

profile of v1, /device:TPU:0, one launch (start us, length us, event | category | flops | bytes accessed | tf_op | source)
XLA Modules:
  0.0 94.4 jit_solution(12300337709441213656)
XLA Ops:
  0.0 92.1 %shard_map.109 = bf16[256,2048]{1,0:T(8,128)(2,1)} custom-call(bf16[1024,2048]{1,0:T(8,128)(2,1)} %tokens_hbm.1, f32[1,2048]{1,0:T(1,128)} %bitcast.1, f32[512,512]{1,0:T(8,128)} %w0_hbm.1, f32[512,512]{1,0:T(8,128)} %w1_hbm.1, f32[512,512]{1,0:T(8,128)} %w2_hbm.1, f32[3,512]{1,0:T(4,128)} %taps_ref.1, f32[512,512]{1,0:T(8,128)} %w3_hbm.1, f32[1,128]{1,0:T(1,128)} %s0_ref.1, ...), custom_call_target="tpu_custom_call" | custom-call | tf_op jit(solution)/shard_map/pallas_call | solution.py:518
  92.1 2.3 %copy.13 = bf16[256,2048]{1,0:T(8,128)(2,1)} copy(bf16[256,2048]{1,0:T(8,128)(2,1)} %shard_map.109) | data formatting | bytes 2097152

commit v2 on v1

--- a/solution.py
+++ b/solution.py
@@ -83,22 +83,25 @@
 MESH = pl.DeviceIdType.MESH
 MATRICES = 3
 EARLY = 2
+LAG = 2
 
 
 def mixer_kernel(
     n,
     tokens_hbm,
-    gain_ref,
+    gain_hbm,
     w0_hbm,
     w1_hbm,
     w2_hbm,
+    taps_hbm,
+    w3_hbm,
+    s0_hbm,
+    s1_hbm,
+    s2_hbm,
+    s3_hbm,
+    out_ref,
+    gain_ref,
     taps_ref,
-    w3_hbm,
-    s0_ref,
-    s1_ref,
-    s2_ref,
-    s3_ref,
-    out_ref,
     toks,
     rows,
     stage,
@@ -111,6 +114,7 @@
     gates_in,
     mixed,
     load_sem,
+    mixer_sem,
     zl_sem,
     zr_sem,
     zin_sem,
@@ -118,7 +122,9 @@
     yin_sem,
     dout_sem,
     din_sem,
-    sout_sem,
+    small_sem,
+    sl_sem,
+    sr_sem,
     sin_sem,
     xout_sem,
     xin_sem,
@@ -137,44 +143,86 @@
     half = block // 2
     seq = rows.shape[0]
     tile = seq // ntp
-    q = s0_ref.shape[1]
-    pieces = EARLY + n
+    q = s0_hbm.shape[1]
+    pieces = EARLY + n + 1
+    last = pieces - 1
     partner = t + 1 - 2 * lax.rem(t, 2)
     across = lax.rem(t + 2, ntp)
     corner = lax.rem(partner + 2, ntp)
     peers = (partner, across, corner)
-    weights = (w0_hbm, w1_hbm, w2_hbm, w3_hbm)
+    weights = (w0_hbm, w1_hbm, w2_hbm)
+
+    barrier = pltpu.get_barrier_semaphore()
+
+    def greet(**target):
+        pl.semaphore_signal(barrier, inc=1, device_id=target, device_id_type=MESH)
+
+    @pl.when(z >= 1)
+    def _():
+        greet(fs=z - 1)
+
+    @pl.when(z <= n - 2)
+    def _():
+        greet(fs=z + 1)
+
+    for peer in peers:
+        greet(tp=peer)
+    greet(grp=1 - y)
+    at_end = (z == 0) | (z == n - 1)
+    greeted = ntp + jnp.where(at_end, 1, 2)
 
     loads = [
-        pltpu.make_async_copy(weights[m], stage.at[m], load_sem.at[m]) for m in range(MATRICES + 1)
+        pltpu.make_async_copy(weights[m], stage.at[m], load_sem.at[m]) for m in range(MATRICES)
     ]
-    token_load = pltpu.make_async_copy(tokens_hbm, toks, load_sem.at[MATRICES + 1])
-    loads[MATRICES].start()
-    for m in range(MATRICES):
-        loads[m].start()
-    token_load.start()
-
-    barrier = pltpu.get_barrier_semaphore()
-    for d in range(1, n):
-        pl.semaphore_signal(
-            barrier, inc=1, device_id={"fs": lax.rem(z + d, n)}, device_id_type=MESH
+
+    def mixer_load(i):
+        c = lax.rem(EARLY * y + i, n)
+        at = pl.ds(pl.multiple_of(c * q, q), q)
+        return pltpu.make_async_copy(
+            w3_hbm.at[at, :], stage.at[MATRICES, at, :], mixer_sem.at[i]
         )
-    for d in range(1, ntp):
-        pl.semaphore_signal(
-            barrier, inc=1, device_id={"tp": lax.rem(t + d, ntp)}, device_id_type=MESH
+
+    def mixer_cast(i):
+        mixer_load(i).wait()
+        c = lax.rem(EARLY * y + i, n)
+        at = pl.ds(pl.multiple_of(c * q, q), q)
+        mix[z, c, t] = stage[MATRICES, at, :].astype(jnp.bfloat16)
+
+    token_load = pltpu.make_async_copy(tokens_hbm, toks, load_sem.at[MATRICES])
+    small = [
+        pltpu.make_async_copy(source, target, small_sem.at[i])
+        for i, (source, target) in enumerate(
+            (
+                (s0_hbm, scales.at[z, :, 0:q]),
+                (s1_hbm, scales.at[z, :, q : 2 * q]),
+                (s2_hbm, scales.at[z, :, 2 * q : 3 * q]),
+                (s3_hbm, scales.at[z, :, 3 * q :]),
+                (gain_hbm, gain_ref),
+                (taps_hbm, taps_ref),
+            )
         )
-    pl.semaphore_signal(barrier, inc=1, device_id={"grp": 1 - y}, device_id_type=MESH)
-
-    scales[z, :, 0:q] = s0_ref[...]
-    scales[z, :, q : 2 * q] = s1_ref[...]
-    scales[z, :, 2 * q : 3 * q] = s2_ref[...]
-    scales[z, :, 3 * q :] = s3_ref[...]
+    ]
+    for i in range(EARLY):
+        mixer_load(i).start()
+    for load in small:
+        load.start()
+    for i in range(EARLY, n):
+        mixer_load(i).start()
+    for load in loads + [token_load]:
+        load.start()
+
+    def depth_of(p, b):
+        c = min(p - EARLY, n - 1)
+        if c < n - 1:
+            return c, b * block, block
+        return c, b * block + (p - EARLY - c) * half, half
 
     def piece(p, b, side):
         if p < EARLY:
             return mix.at[b, EARLY * side + p, t]
-        first = pl.multiple_of(b * block + side * half, half)
-        return held.at[p - EARLY, pl.ds(first, half), :]
+        c, first, count = depth_of(p, b)
+        first = pl.multiple_of(first + side * (count // 2), count // 2)
+        return held.at[c, pl.ds(first, count // 2), :]
 
     def remote(ref, send, recv, target):
         return pltpu.make_async_remote_copy(
@@ -199,34 +247,87 @@
         return remote(piece(p, b, 1 - y), yout_sem.at[p, b], yin_sem.at[p, b], {"grp": 1 - y})
 
     inward = jnp.where(z == 0, 1, n - 2)
-
-    def second_half(p, b):
-        return remote(piece(p, b, 1 - y), dout_sem.at[p], din_sem.at[p], {"fs": inward})
-
-    def direct(b):
-        return ((z == 1) & (b == 0)) | ((z == n - 2) & (b == n - 1))
-
-    at_end = (z == 0) | (z == n - 1)
-
-    def scale_copy(d):
-        return remote(scales.at[z], sout_sem.at[d], sin_sem.at[z], {"fs": lax.rem(z + d, n)})
-
-    def scale_arrival(d):
-        source = lax.rem(z + d, n)
-        return remote(scales.at[source], sout_sem.at[d], sin_sem.at[source], {"fs": source})
+    outward = jnp.where(z <= 1, 0, n - 1)
+    edge = jnp.where(z <= 1, 0, n - 1)
+
+    def second_half(p):
+        return remote(piece(p, edge, 1 - y), dout_sem.at[p], din_sem.at[p], {"fs": inward})
+
+    next_in = jnp.where(z <= 1, 1, n - 2)
+
+    def final_half():
+        return remote(
+            piece(last, next_in, 1 - y), dout_sem.at[pieces], din_sem.at[pieces], {"fs": outward}
+        )
+
+    inside = jnp.logical_not(at_end)
+
+    def from_edge(b):
+        return inside & (b == edge)
+
+    def from_inside(p, b):
+        return at_end & (b == next_in) & (p == last)
+
+    def by_twin(p, b):
+        return jnp.logical_not(from_edge(b) | from_inside(p, b))
+
+    def scale_left(b):
+        return remote(scales.at[b], sl_sem.at[b], sin_sem.at[b], {"fs": z - 1})
+
+    def scale_right(b):
+        return remote(scales.at[b], sr_sem.at[b], sin_sem.at[b], {"fs": z + 1})
+
+    def send_scales():
+        @pl.when(z >= 1)
+        def _():
+            scale_left(z).start()
+
+        @pl.when(z <= n - 2)
+        def _():
+            scale_right(z).start()
+
+    def relay_scales(s):
+        from_right, from_left = z + 1 + s, z - 1 - s
+
+        @pl.when(from_right <= n - 1)
+        def _():
+            scale_left(from_right).wait_recv()
+
+            @pl.when(z >= 1)
+            def _():
+                scale_left(from_right).start()
+
+        @pl.when(from_left >= 0)
+        def _():
+            scale_right(from_left).wait_recv()
+
+            @pl.when(z <= n - 2)
+            def _():
+                scale_right(from_left).start()
 
     def send_own(p):
-        @pl.when(z >= 1)
+        keep = inside & (p == last)
+
+        @pl.when((z >= 1) & jnp.logical_not(keep & (outward == 0)))
         def _():
             to_left(p, z).start()
 
-        @pl.when(z <= n - 2)
+        @pl.when((z <= n - 2) & jnp.logical_not(keep & (outward == n - 1)))
         def _():
             to_right(p, z).start()
 
-        @pl.when(at_end)
-        def _():
-            second_half(p, z).start()
+    def send_final():
+        @pl.when(inside & (outward == 0))
+        def _():
+            to_left(last, z).start()
+
+        @pl.when(inside & (outward == n - 1))
+        def _():
+            to_right(last, z).start()
+
+        @pl.when(inside)
+        def _():
+            final_half().start()
 
     def relay(p, s):
         from_right, from_left = z + 1 + s, z - 1 - s
@@ -239,7 +340,7 @@
             def _():
                 to_left(p, from_right).start()
 
-            @pl.when(jnp.logical_not(direct(from_right)))
+            @pl.when(by_twin(p, from_right))
             def _():
                 to_twin(p, from_right).start()
 
@@ -251,16 +352,22 @@
             def _():
                 to_right(p, from_left).start()
 
-            @pl.when(jnp.logical_not(direct(from_left)))
+            @pl.when(by_twin(p, from_left))
             def _():
                 to_twin(p, from_left).start()
 
     def second_arrived(p, b):
-        @pl.when(direct(b))
-        def _():
-            second_half(p, b).wait_recv()
-
-        @pl.when(jnp.logical_not(direct(b)))
+        @pl.when(from_edge(b))
+        def _():
+            second_half(p).wait_recv()
+
+        if p == last:
+
+            @pl.when(from_inside(p, b))
+            def _():
+                final_half().wait_recv()
+
+        @pl.when(by_twin(p, b))
         def _():
             from_twin(p, b).wait_recv()
 
@@ -307,17 +414,17 @@
         across_arrival(b).wait_recv()
         core_relay(b).start()
 
-    def multiply(c, b, first_time=False):
-        at = pl.ds(pl.multiple_of(b * block, block), block)
+    def multiply(c, first, count, first_time=False):
+        at = pl.ds(pl.multiple_of(first, count), count)
         for i in range(2):
             r = slice(i * seq // 2, (i + 1) * seq // 2)
             part = jnp.dot(rows[r, at], held[c, at, :], preferred_element_type=jnp.float32)
             acc[c, r, :] = part if first_time else acc[c, r, :] + part
 
-    def multiply_arrived(c, s):
+    def multiply_arrived(p, s):
         def act(b):
-            second_arrived(EARLY + c, b)
-            multiply(c, b)
+            second_arrived(p, b)
+            multiply(*depth_of(p, b))
 
         each_block(s, act)
 
@@ -357,21 +464,21 @@
         for k in range(ntp - 1):
             gate_arrival(c, k).wait_recv()
 
-    def mix_chunks(first, last, final):
-        count = last - first
+    def mix_chunks(first, stop):
+        count = stop - first
         left = jnp.concatenate(
-            [gates_in[c, k] for c in range(first, last) for k in range(ntp)], axis=1
+            [gates_in[c, k] for c in range(first, stop) for k in range(ntp)], axis=1
         )
         for b in range(n):
             cols = slice(b * block, (b + 1) * block)
-            right = mix[b, first:last].reshape(count * ntp * q, block)
+            right = mix[b, first:stop].reshape(count * ntp * q, block)
             part = jnp.dot(left, right, preferred_element_type=jnp.float32)
-            if final:
-                out_ref[:, cols] = ((mixed[:, cols] + part) * scales[b, :, 3 * q :]).astype(
-                    jnp.bfloat16
-                )
+            if first > 0:
+                part = mixed[:, cols] + part
+            if stop < n:
+                mixed[:, cols] = part
             else:
-                mixed[:, cols] = part
+                out_ref[:, cols] = (part * scales[b, :, 3 * q :]).astype(jnp.bfloat16)
 
     def mix_in():
         @pl.loop(0, n)
@@ -385,14 +492,17 @@
         at = slice(i * strip, (i + 1) * strip)
         rows[at, :] = normed(toks[at, :], gain_ref[...])
 
-    loads[MATRICES].wait()
-    for c in range(n):
-        mix[z, c, t] = stage[MATRICES, c * q : (c + 1) * q, :].astype(jnp.bfloat16)
-    pl.semaphore_wait(barrier, n - 1 + ntp - 1 + 1)
-    for p in range(EARLY):
+    for i in range(EARLY):
+        mixer_cast(i)
+    pl.semaphore_wait(barrier, greeted)
+    send_own(0)
+    for load in small:
+        load.wait()
+    send_scales()
+    for p in range(1, EARLY):
         send_own(p)
-    for d in range(1, n):
-        scale_copy(d).start()
+    for i in range(EARLY, n):
+        mixer_cast(i)
     spread(z)
     for m in range(MATRICES):
         loads[m].wait()
@@ -404,76 +514,100 @@
 
     @pl.when(at_end)
     def _():
+        for p in range(EARLY):
+            second_half(p).start()
         for p in range(EARLY, pieces):
             send_own(p)
+            second_half(p).start()
 
     def send_own_inside(p):
-        @pl.when(jnp.logical_not(at_end))
+        @pl.when(inside)
         def _():
             send_own(p)
 
     token_load.wait()
 
     def own_part(c):
-        multiply(c, z, True)
-
-    def scales_in():
-        for d in range(1, n):
-            scale_arrival(d).wait_recv()
+        multiply(c, z * block, block, True)
 
     part = functools.partial
     hops = n - 1
-    work = {k: [] for k in range(pieces * hops)}
+    order = [(0, 0), (1, 0), (0, 1), (1, 1), (0, 2), (2, 0), (1, 2), (2, 1), (2, 2)]
+    order += [(p, s) for p in range(EARLY + 1, last) for s in range(hops)]
+    work = {k: [] for k in range(len(order))}
     for i in range(8):
         work[i // 2].append(part(normalise, i))
     for c in range(n):
         work[4 + c // 2].append(part(own_part, c))
     for s in range(hops):
-        work[hops * EARLY - 1 + s].append(part(spread_arrived, s))
-    work[7].append(scales_in)
-    for c in range(n):
-        for s in range(hops):
-            at = (EARLY + c) * hops + s + 1
-            if at in work:
-                work[at].append(part(multiply_arrived, c, s))
-                if s == hops - 1:
-                    work[at].append(part(gate, c))
+        work[(1, 4, 8)[s]].append(part(relay_scales, s))
+        work[order.index((EARLY - 1, s)) + LAG].append(part(spread_arrived, s))
+    later = []
+    for k, (p, s) in enumerate(order):
+        if p >= EARLY:
+            tasks = work[k + LAG] if k + LAG < len(order) else later
+            tasks.append(part(multiply_arrived, p, s))
+            if s == hops - 1 and p - EARLY < n - 1:
+                tasks.append(part(gate, p - EARLY))
     work[9].append(lambda: pass_on(z))
-    work[12].append(lambda: each_block(0, pass_on))
-    work[14].append(lambda: each_block(1, pass_on))
-    work[15].append(lambda: each_block(2, pass_on))
-    work[16] += [mix_in, part(gates_arrived, 0), part(gates_arrived, 1), part(mix_chunks, 0, 2, False)]
-
-    for k in range(pieces * hops):
-        p, s = divmod(k, hops)
+    work[13].append(lambda: each_block(0, pass_on))
+    work[16].append(lambda: each_block(1, pass_on))
+    work[17].append(lambda: each_block(2, pass_on))
+
+    for k, (p, s) in enumerate(order):
         relay(p, s)
-        if s == n - 3 and p + 1 < pieces and p + 1 >= EARLY:
-            send_own_inside(p + 1)
+        if s == 1 and p != 1:
+            send_own_inside(max(p + 1, EARLY))
         for task in work[k]:
             task()
-    multiply_arrived(n - 1, hops - 1)
+
+    @pl.when(inside)
+    def _():
+        relay(last, 0)
+
+    relay(last, 1)
+    send_final()
+    for task in later:
+        task()
+    relay(last, 2)
+    mix_in()
+    for c in range(EARLY):
+        gates_arrived(c)
+    mix_chunks(0, EARLY)
+    multiply_arrived(last, 1)
+    multiply_arrived(last, 2)
+
+    @pl.when(at_end)
+    def _():
+        relay(last, 0)
+
+    multiply_arrived(last, 0)
     gate(n - 1)
     gates_arrived(n - 2)
-    gates_arrived(n - 1)
-    mix_chunks(n - 2, n, True)
-
-    for d in range(1, n):
-        scale_copy(d).wait_send()
-    for c in range(n):
-        for k in range(ntp - 1):
-            gate_copy(c, k).wait_send()
-
+    mix_chunks(n - 2, n - 1)
     @pl.loop(0, n)
     def _(b):
         across_copy(b).wait_send()
         core_copy(b).wait_send()
         core_relay(b).wait_send()
 
+        @pl.when((b >= z) & (z >= 1))
+        def _():
+            scale_left(b).wait_send()
+
+        @pl.when((b <= z) & (z <= n - 2))
+        def _():
+            scale_right(b).wait_send()
+
+    @pl.when(inside)
+    def _():
+        final_half().wait_send()
+
     for p in range(pieces):
 
         @pl.when(at_end)
         def _():
-            second_half(p, z).wait_send()
+            second_half(p).wait_send()
 
         @pl.loop(0, n)
         def _(b):
@@ -485,9 +619,16 @@
             def _():
                 to_right(p, b).wait_send()
 
-            @pl.when((b != z) & jnp.logical_not(direct(b)))
+            @pl.when((b != z) & by_twin(p, b))
             def _():
                 to_twin(p, b).wait_send()
+
+    gates_arrived(n - 1)
+    mix_chunks(n - 1, n)
+
+    for c in range(n):
+        for k in range(ntp - 1):
+            gate_copy(c, k).wait_send()
 
 
 def fused_device(
@@ -509,30 +650,19 @@
     block, width = outer_weight.shape
     tile = seq // ntp
     q = outer_scale.shape[1]
-    pieces = EARLY + n
-    whole = pl.BlockSpec(memory_space=pltpu.VMEM)
+    pieces = EARLY + n + 1
     anywhere = pl.BlockSpec(memory_space=pl.ANY)
     bf16, f32 = jnp.bfloat16, jnp.float32
     dma = pltpu.SemaphoreType.DMA
     scale_width = 3 * q + mixer_scale.shape[1]
     return pl.pallas_call(
         functools.partial(mixer_kernel, n),
-        out_shape=jax.ShapeDtypeStruct((tile, n * block), bf16),
-        in_specs=[
-            anywhere,
-            whole,
-            anywhere,
-            anywhere,
-            anywhere,
-            whole,
-            anywhere,
-            whole,
-            whole,
-            whole,
-            whole,
-        ],
-        out_specs=whole,
+        out_shape=pltpu.VMEM((tile, n * block), bf16),
+        in_specs=[anywhere] * 11,
+        out_specs=pl.BlockSpec(memory_space=pltpu.VMEM),
         scratch_shapes=[
+            pltpu.VMEM((1, depth), f32),
+            pltpu.VMEM(filter_taps.shape, f32),
             pltpu.VMEM((seq, depth), bf16),
             pltpu.VMEM((seq, depth), bf16),
             pltpu.VMEM((MATRICES + 1, block, width), f32),
@@ -544,14 +674,17 @@
             pltpu.VMEM((n, seq, q), bf16),
             pltpu.VMEM((n, ntp, tile, q), bf16),
             pltpu.VMEM((tile, n * block), f32),
-            dma((MATRICES + 2,)),
+            dma((MATRICES + 1,)),
+            dma((n,)),
             dma((pieces, n)),
             dma((pieces, n)),
             dma((pieces, n)),
             dma((pieces, n)),
             dma((pieces, n)),
-            dma((pieces,)),
-            dma((pieces,)),
+            dma((pieces + 1,)),
+            dma((pieces + 1,)),
+            dma((6,)),
+            dma((n,)),
             dma((n,)),
             dma((n,)),
             dma((n,)),

time: 94.7 us -> 87.9 us (0.928)
  Pallas kernels: 92.1 us -> 86.7 us
  local copies, waits for them, and re-layouts: 2.3 us -> 0.97 us
    pallas_call x1, Pallas kernels: 92.1 us -> 86.7 us  [fused_device(): pl.pallas_call(functools.partial(mixer_kernel, n), out_shape=pltpu.VMEM((...]
    unnamed x1, local copies, waits for them, and re-layouts: 2.3 us -> 0.97 us
where the time goes in v2:
time: 87.9 us; the launch traced here: 87.7 us
  Pallas kernels  86.7 us (99%)
  local copies, waits for them, and re-layouts  0.97 us (1%)
    pallas_call x1, Pallas kernels, fused_device(): pl.pallas_call(functools.partial(mixer_kernel, n), out_shape=pltpu.VMEM((...  86.7 us

profile of v2, /device:TPU:0, one launch (start us, length us, event | category | flops | bytes accessed | tf_op | source)
XLA Modules:
  0.0 87.7 jit_solution(11165735293100321499)
XLA Ops:
  0.0 86.7 %shard_map.109 = bf16[256,2048]{1,0:T(8,128)(2,1)S(1)} custom-call(bf16[1024,2048]{1,0:T(8,128)(2,1)} %tokens_hbm.1, f32[1,2048]{1,0:T(1,128)} %bitcast.1, f32[512,512]{1,0:T(8,128)} %w0_hbm.1, f32[512,512]{1,0:T(8,128)} %w1_hbm.1, f32[512,512]{1,0:T(8,128)} %w2_hbm.1, f32[3,512]{1,0:T(4,128)} %taps_hbm.1, f32[512,512]{1,0:T(8,128)} %w3_hbm.1, ...), custom_call_target="tpu_custom_call" | custom-call | tf_op jit(solution)/shard_map/pallas_call | solution.py:658
  86.7 1.0 %copy.13 = bf16[256,2048]{1,0:T(8,128)(2,1)} copy(bf16[256,2048]{1,0:T(8,128)(2,1)S(1)} %shard_map.109) | data formatting | bytes 2097152
